TPU v7x, 32 devices: a whole 2x2x4 slice. The times are simulated.
32 devices in a mesh: kv: 8 (over z, x), tp: 4 (over y, core).
Axes of the slice: x: 2, y: 2, z: 4, core: 2. Of those that a mesh axis runs over, the one named last changes fastest.
Arguments:
- tokens: bfloat16 [8192, 2048], P('kv'), may hold values from -72 to 72
- query_weight: bfloat16 [2048, 2048], P(None, 'tp'), may hold values from -0.125 to 0.125
- key_projection_matrix: bfloat16 [2048, 1024], P(None, 'tp'), may hold values from -0.125 to 0.125
- value_projection_matrix: bfloat16 [2048, 1024], P(None, 'tp'), may hold values from -0.125 to 0.125
- out_weight: bfloat16 [2048, 2048], P('tp'), may hold values from -1.5 to 1.5
- chosen: int32 [64, 12], P('kv'), may hold values from -1 to 255, as said below
Outputs:
- layer_out: bfloat16 [8192, 2048], P(('kv', 'tp'))
Inputs may be any that keep to these rules, and one draw needn't show every extreme that they name: `chosen`: positions are grouped in consecutive groups of 1024. The blocks named in one row lie in distinct groups, all earlier than the group of the row's query block; a query block in group g has exactly min(12, g) entries that are not -1, first in its row, and the rest are -1. So the query blocks of one group name at most 8 blocks of any one other group, and in every draw some group's query blocks all name blocks of one same earlier group.
All inputs are finite; a program needn't handle non-finite values.
Results may differ from a plain program's by a relative error of at most 0.014.
The roundings to bfloat16 on the way count: a program that leaves them out, or rounds other values in their place, can miss the bound.
Values may be sent and summed in bfloat16 or wider, within the bound.
A program may use at most 64 MiB of HBM per device.

v0:
```python
import jax
import jax.numpy as jnp
from jax import lax
from jax.sharding import PartitionSpec as P

HEAD_SIZE = 128
QUERY_BLOCK_SPAN = 128
KEY_BLOCK_SPAN = 32
NFAR = 12


def shards(
    tokens, query_weight, key_projection_matrix, value_projection_matrix, out_weight, chosen
):
    tok_rows = tokens.shape[0]
    kv_width = key_projection_matrix.shape[1]
    kv_heads = kv_width // HEAD_SIZE
    q_heads = query_weight.shape[1] // HEAD_SIZE
    grouped_head_index = q_heads // kv_heads
    query_blocks = tok_rows // QUERY_BLOCK_SPAN
    blocked_keys = tok_rows // KEY_BLOCK_SPAN
    queries = jnp.dot(tokens, query_weight, preferred_element_type=jnp.float32).astype(jnp.bfloat16)
    key_vectors = jnp.dot(tokens, key_projection_matrix, preferred_element_type=jnp.float32).astype(
        jnp.bfloat16
    )
    value_vectors = jnp.dot(
        tokens, value_projection_matrix, preferred_element_type=jnp.float32
    ).astype(jnp.bfloat16)
    my_index = lax.axis_index("kv")
    key_rows = key_vectors.reshape(blocked_keys, KEY_BLOCK_SPAN, kv_width)
    value_rows = value_vectors.reshape(blocked_keys, KEY_BLOCK_SPAN, kv_width)
    all_lists = lax.all_gather(chosen, "kv", axis=0, tiled=True)
    peer_count = all_lists.shape[0] // query_blocks
    asked_ids = all_lists.reshape(peer_count, query_blocks, NFAR)
    is_mine = (asked_ids >= 0) & (asked_ids // blocked_keys == my_index)
    wanted = jnp.sum(jnp.where(is_mine, asked_ids - my_index * blocked_keys, 0), axis=2)
    received = (
        lax.all_to_all(key_rows[wanted], "kv", split_axis=0, concat_axis=0, tiled=True),
        lax.all_to_all(value_rows[wanted], "kv", split_axis=0, concat_axis=0, tiled=True),
    )
    owners = jnp.where(chosen >= 0, chosen // blocked_keys, 0)
    block_slot = jnp.arange(query_blocks, dtype=jnp.int32)[:, None]
    far_keys = received[0][owners, block_slot]
    far_values = received[1][owners, block_slot]
    listed_keys = QUERY_BLOCK_SPAN + NFAR * KEY_BLOCK_SPAN
    row_offset = my_index * tok_rows
    query_pos = row_offset + jnp.arange(tok_rows, dtype=jnp.int32).reshape(
        query_blocks, QUERY_BLOCK_SPAN
    )
    far_pos = (
        jnp.maximum(chosen, 0)[:, :, None] * KEY_BLOCK_SPAN
        + jnp.arange(KEY_BLOCK_SPAN, dtype=jnp.int32)
    ).reshape(query_blocks, NFAR * KEY_BLOCK_SPAN)
    far_ok = jnp.broadcast_to(
        (chosen >= 0)[:, :, None], (query_blocks, NFAR, KEY_BLOCK_SPAN)
    ).reshape(query_blocks, NFAR * KEY_BLOCK_SPAN)
    key_pos = jnp.concatenate([query_pos, far_pos], axis=1)
    key_ok = jnp.concatenate(
        [jnp.ones((query_blocks, QUERY_BLOCK_SPAN), dtype=bool), far_ok], axis=1
    )
    allowed = key_ok[:, None, :] & (key_pos[:, None, :] <= query_pos[:, :, None])
    all_keys = jnp.concatenate(
        [
            key_vectors.reshape(query_blocks, QUERY_BLOCK_SPAN, kv_width),
            far_keys.reshape(query_blocks, NFAR * KEY_BLOCK_SPAN, kv_width),
        ],
        axis=1,
    )
    all_values = jnp.concatenate(
        [
            value_vectors.reshape(query_blocks, QUERY_BLOCK_SPAN, kv_width),
            far_values.reshape(query_blocks, NFAR * KEY_BLOCK_SPAN, kv_width),
        ],
        axis=1,
    )
    grouped = queries.reshape(
        query_blocks, QUERY_BLOCK_SPAN, kv_heads, grouped_head_index, HEAD_SIZE
    )
    scores = jnp.einsum(
        "bqgrd,bkgd->bgrqk",
        grouped,
        all_keys.reshape(query_blocks, listed_keys, kv_heads, HEAD_SIZE),
        preferred_element_type=jnp.float32,
    ) * HEAD_SIZE ** (-0.5)
    scores = jnp.where(allowed[:, None, None], scores, -jnp.inf)
    row_max = jnp.max(scores, axis=-1, keepdims=True)
    exp_scores = jnp.exp(scores - row_max)
    row_sum = jnp.sum(exp_scores, axis=-1, keepdims=True)
    weights = (exp_scores / row_sum).astype(jnp.bfloat16)
    mixed = jnp.einsum(
        "bgrqk,bkgd->bqgrd",
        weights,
        all_values.reshape(query_blocks, listed_keys, kv_heads, HEAD_SIZE),
        preferred_element_type=jnp.float32,
    )
    mixed = mixed.astype(jnp.bfloat16).reshape(tok_rows, q_heads * HEAD_SIZE)
    return lax.psum_scatter(
        jnp.dot(mixed, out_weight, preferred_element_type=jnp.float32).astype(jnp.bfloat16),
        "tp",
        scatter_dimension=0,
        tiled=True,
    )


def solution(mesh):
    return jax.shard_map(
        shards,
        mesh=mesh,
        in_specs=(
            P("kv", None),
            P(None, "tp"),
            P(None, "tp"),
            P(None, "tp"),
            P("tp", None),
            P("kv", None),
        ),
        out_specs=P(("kv", "tp"), None),
        check_vma=False,
    )
```

profile of v0, /device:TPU:21, one launch (start us, length us, event | category | flops | bytes accessed | tf_op | source)
XLA Modules:
  0.0 182.3 jit_solution(7131754344731125927)
XLA Ops:
  6.5 20.1 %all_gather.3 = s32[64,12]{1,0:T(8,128)S(1)} all-gather(s32[8,12]{1,0:T(8,128)} %param.11), channel_id=1, replica_groups=mesh['kv'=8,'tp'=4] {'kv'}, dimensions={0}, use_global_device_ids=true | all-gather | bytes 3456 | tf_op jit(solution)/shard_map/all_gather | solution.py:32
  26.7 0.1 select_reduce_fusion
  26.9 0.1 reshape.100
  27.0 3.7 %convolution_convert_fusion.2 = bf16[1024,256]{1,0:T(8,128)(2,1)S(1)} fusion(bf16[1024,2048]{1,0:T(8,128)(2,1)} %param.6, bf16[2048,256]{1,0:T(8,128)(2,1)} %param.8), kind=kOutput, calls=%fused_computation.25 | convolution fusion | flops 1074003968 | bytes 5767168 | tf_op jit(solution)/shard_map/dot_general | solution.py:23
  30.7 1.6 gather_fusion.2
  32.3 10.0 %all-to-all-start.1 = ((bf16[8,8,32,256]{3,2,1,0:T(8,128)(2,1)}), bf16[8,8,32,256]{3,2,1,0:T(8,128)(2,1)S(1)}, u32[]{:S(2)}, u32[]{:S(2)}) async-start(bf16[8,8,32,256]{3,2,1,0:T(8,128)(2,1)} %bitcast.56), calls=%async_computation.1 | async-start | bytes 2097152 | tf_op jit(solution)/shard_map/all_to_all | solution.py:38
  42.3 4.6 %convolution_convert_fusion.3 = bf16[1024,256]{1,0:T(8,128)(2,1)} fusion(bf16[1024,2048]{1,0:T(8,128)(2,1)} %param.6, bf16[2048,256]{1,0:T(8,128)(2,1)} %param.9), kind=kOutput, calls=%fused_computation.26 | convolution fusion | flops 1074003968 | bytes 5767168 | tf_op jit(solution)/shard_map/dot_general | solution.py:26
  46.8 2.6 %gather_fusion = bf16[64,32,256]{2,1,0:T(8,128)(2,1)} fusion(bf16[32,32,256]{2,1,0:T(8,128)(2,1)} %bitcast.54, s32[1024]{0:T(1024)S(1)} %pad_clamp_fusion), kind=kCustom, calls=%fused_computation | custom fusion | bytes 2097408 | tf_op jit(solution)/shard_map/gather | solution.py:39
  49.5 12.4 %all-to-all-done.1 = bf16[8,8,32,256]{3,2,1,0:T(8,128)(2,1)S(1)} async-done(((bf16[8,8,32,256]{3,2,1,0:T(8,128)(2,1)}), bf16[8,8,32,256]{3,2,1,0:T(8,128)(2,1)S(1)}, u32[]{:S(2)}, u32[]{:S(2)}) %all-to-all-start.1) | async-done | bytes 1048608 | tf_op jit(solution)/shard_map/all_to_all | solution.py:38
  61.9 7.0 %all-to-all-start = ((bf16[8,8,32,256]{3,2,1,0:T(8,128)(2,1)}), bf16[8,8,32,256]{3,2,1,0:T(8,128)(2,1)}, u32[]{:S(2)}, u32[]{:S(2)}) async-start(bf16[8,8,32,256]{3,2,1,0:T(8,128)(2,1)} %bitcast.55), calls=%async_computation | async-start | bytes 2097152 | tf_op jit(solution)/shard_map/all_to_all | solution.py:39
  68.9 2.0 %concatenate.32 = bf16[8,128,2,128]{3,2,1,0:T(2,128)(2,1)} reshape(bf16[1024,256]{1,0:T(8,128)(2,1)} %copy-done.1) | data formatting | bytes 1048576 | tf_op jit(solution)/shard_map/concatenate | solution.py:62
  70.9 1.9 %concatenate.26 = bf16[8,128,2,128]{3,2,1,0:T(2,128)(2,1)} reshape(bf16[1024,256]{1,0:T(8,128)(2,1)} %convolution_convert_fusion.3) | data formatting | bytes 1048576 | tf_op jit(solution)/shard_map/concatenate | solution.py:69
  72.9 2.0 %copy.13 = bf16[8,128,2,128]{3,1,2,0:T(8,128)(2,1)} copy(bf16[8,128,2,128]{3,2,1,0:T(2,128)(2,1)} %concatenate.32) | data formatting | bytes 1048576 | tf_op jit(solution)/shard_map/concatenate | solution.py:62
  74.9 6.2 %convolution_convert_fusion.1 = bf16[1024,512]{1,0:T(8,128)(2,1)} fusion(bf16[1024,2048]{1,0:T(8,128)(2,1)} %param.6, bf16[2048,512]{1,0:T(8,128)(2,1)} %param.7), kind=kOutput, calls=%fused_computation.23 | convolution fusion | flops 2148007936 | bytes 7340032 | tf_op jit(solution)/shard_map/dot_general | solution.py:22
  81.0 2.2 %reshape.96 = bf16[8,128,2,2,128]{4,3,2,1,0:T(2,128)(2,1)} reshape(bf16[1024,512]{1,0:T(8,128)(2,1)} %convolution_convert_fusion.1) | data formatting | bytes 2097152 | tf_op jit(solution)/shard_map/reshape | solution.py:76
  83.3 0.1 add.62
  83.5 0.1 broadcast_in_dim.20
  83.6 0.1 reshape.91
  83.7 2.0 %copy.11 = bf16[8,128,2,128]{1,3,2,0:T(8,128)(2,1)} copy(bf16[8,128,2,128]{3,2,1,0:T(2,128)(2,1)} %concatenate.26) | data formatting | bytes 1048576 | tf_op jit(solution)/shard_map/concatenate | solution.py:69
  85.7 2.4 %compare_and_fusion = pred[8,128,512]{1,2,0:T(8,128)(4,1)} fusion(s32[8,128]{1,0:T(8,128)S(1)} %add_add_fusion, s32[8,512]{1,0:T(8,128)S(1)} %pad_add_fusion, pred[8,512]{1,0:T(8,128)(4,1)S(1)} %concatenate.30), kind=kLoop, calls=%fused_computation.21 | loop fusion | flops 1048576 | bytes 548864 | tf_op jit(solution)/shard_map/and | solution.py:61
  88.0 2.3 %gather_fusion.3 = bf16[96,32,256]{2,1,0:T(8,128)(2,1)} fusion(bf16[8,8,32,256]{3,2,1,0:T(8,128)(2,1)S(1)} %all-to-all-done.1, s32[96]{0:T(128)S(1)} %reshape.106), kind=kCustom, calls=%fused_computation.3 | custom fusion | bytes 3146496 | tf_op jit(solution)/shard_map/gather | solution.py:43
  90.4 3.5 %concatenate.33 = bf16[8,384,2,128]{3,2,1,0:T(2,128)(2,1)} reshape(bf16[96,32,256]{2,1,0:T(8,128)(2,1)} %gather_fusion.3) | data formatting | bytes 3145728 | tf_op jit(solution)/shard_map/concatenate | solution.py:62
  93.9 2.9 %copy.14 = bf16[8,384,2,128]{3,1,2,0:T(8,128)(2,1)} copy(bf16[8,384,2,128]{3,2,1,0:T(2,128)(2,1)} %concatenate.33) | data formatting | bytes 3145728 | tf_op jit(solution)/shard_map/concatenate | solution.py:62
  96.8 3.6 %gather_fusion.1 = bf16[96,32,256]{2,1,0:T(8,128)(2,1)} fusion(bf16[8,8,32,256]{3,2,1,0:T(8,128)(2,1)} %all-to-all-done, s32[96]{0:T(128)S(1)} %reshape.106), kind=kCustom, calls=%fused_computation.1 | custom fusion | bytes 3146496 | tf_op jit(solution)/shard_map/gather | solution.py:44
  100.4 3.5 %concatenate.28 = bf16[8,384,2,128]{3,2,1,0:T(2,128)(2,1)} reshape(bf16[96,32,256]{2,1,0:T(8,128)(2,1)} %gather_fusion.1) | data formatting | bytes 3145728 | tf_op jit(solution)/shard_map/concatenate | solution.py:69
  103.9 4.9 %copy.12 = bf16[8,384,2,128]{1,3,2,0:T(8,128)(2,1)} copy(bf16[8,384,2,128]{3,2,1,0:T(2,128)(2,1)} %concatenate.28) | data formatting | bytes 3145728 | tf_op jit(solution)/shard_map/concatenate | solution.py:69
  108.9 2.8 %fusion.8 = f32[8,2,512,128,2]{3,2,4,1,0:T(8,128)S(1)} fusion(bf16[8,384,2,128]{3,1,2,0:T(8,128)(2,1)} %copy.14, bf16[8,128,2,128]{3,1,2,0:T(8,128)(2,1)} %copy.13, bf16[8,128,2,2,128]{4,3,2,1,0:T(2,128)(2,1)S(1)} %copy-done.2), kind=kOutput, calls=%fused_computation.18 | convolution fusion | flops 541065216 | bytes 11534336 | tf_op jit(solution)/shard_map/bqgrd,bkgd->bgrqk/dot_general | solution.py:79
  111.7 5.8 %fusion.30 = (f32[8,2,2,128]{3,2,1,0:T(2,128)S(1)}, f32[8,2,2,128,512]{3,4,2,1,0:T(8,128)}) fusion(f32[8,2,512,128,2]{3,2,4,1,0:T(8,128)S(1)} %fusion.8, pred[8,128,512]{1,2,0:T(8,128)(4,1)S(1)} %copy-done.5), kind=kOutput, calls=%fused_computation.63 | output fusion | flops 12583423 | bytes 17317888 | tf_op jit(solution)/shard_map/sub | solution.py:87
  117.5 4.3 %fusion.12 = bf16[8,128,2,2,128]{1,4,3,2,0:T(8,128)(2,1)S(1)} fusion(f32[8,2,2,128,512]{3,4,2,1,0:T(8,128)} %get-tuple-element.6, f32[8,2,2,128]{3,2,1,0:T(2,128)S(1)} %get-tuple-element.5, bf16[8,384,2,128]{1,3,2,0:T(8,128)(2,1)S(1)} %copy-done.3, bf16[8,128,2,128]{1,3,2,0:T(8,128)(2,1)S(1)} %copy-done.4), kind=kOutput, calls=%fused_computation.24 | convolution fusion | flops 545783808 | bytes 11550720 | tf_op jit(solution)/shard_map/bgrqk,bkgd->bqgrd/dot_general | solution.py:90
  121.8 0.7 copy.17
  122.5 4.3 %convolution_convert_fusion = bf16[1024,2048]{1,0:T(8,128)(2,1)} fusion(bf16[512,2048]{1,0:T(8,128)(2,1)S(1)} %copy-done, bf16[64,8,8,128]{3,2,1,0:T(8,128)(2,1)S(1)} %bitcast.57), kind=kOutput, calls=%fused_computation.13 | convolution fusion | flops 2149580800 | bytes 7340032 | tf_op jit(solution)/shard_map/dot_general | solution.py:98
  126.9 48.6 %reduce-scatter.2.cloned.1.call-done = bf16[256,2048]{1,0:T(8,128)(2,1)} async-done(((bf16[1024,2048]{1,0:T(8,128)(2,1)}), bf16[256,2048]{1,0:T(8,128)(2,1)}) %reduce-scatter.2.cloned.1.call-update) | async-done | bytes 1048592 | tf_op jit(solution)/shard_map/reduce_scatter | solution.py:97
  (31 shorter events, 0.4 us)
Async XLA Ops:
  6.5 116.0 %copy-start = (bf16[512,2048]{1,0:T(8,128)(2,1)S(1)}, bf16[512,2048]{1,0:T(8,128)(2,1)}, u32[]{:S(2)}) copy-start(bf16[512,2048]{1,0:T(8,128)(2,1)} %param.10) | copy-start | bytes 6291460
  30.7 1.6 copy-start.1
  32.3 29.6 %all-to-all-start.1 = ((bf16[8,8,32,256]{3,2,1,0:T(8,128)(2,1)}), bf16[8,8,32,256]{3,2,1,0:T(8,128)(2,1)S(1)}, u32[]{:S(2)}, u32[]{:S(2)}) async-start(bf16[8,8,32,256]{3,2,1,0:T(8,128)(2,1)} %bitcast.56), calls=%async_computation.1 | async-start | bytes 2097152 | tf_op jit(solution)/shard_map/all_to_all | solution.py:38
  42.3 26.6 %copy-start.6 = (s32[8,12]{1,0:T(8,128)S(1)}, s32[8,12]{1,0:T(8,128)}, u32[]{:S(2)}) copy-start(s32[8,12]{1,0:T(8,128)} %param.11) | copy-start | bytes 1156
  61.9 34.9 %all-to-all-start = ((bf16[8,8,32,256]{3,2,1,0:T(8,128)(2,1)}), bf16[8,8,32,256]{3,2,1,0:T(8,128)(2,1)}, u32[]{:S(2)}, u32[]{:S(2)}) async-start(bf16[8,8,32,256]{3,2,1,0:T(8,128)(2,1)} %bitcast.55), calls=%async_computation | async-start | bytes 2097152 | tf_op jit(solution)/shard_map/all_to_all | solution.py:39
  68.9 106.6 %reduce-scatter.2.cloned.1.call-start = ((), (), s32[]{:S(2)}) async-start(), calls=%async_computation.3 | async-start | bytes 5242880 | tf_op jit(solution)/shard_map/reduce_scatter | solution.py:97
  96.8 12.1 %copy-start.2 = (bf16[8,128,2,2,128]{4,3,2,1,0:T(2,128)(2,1)S(1)}, bf16[8,128,2,2,128]{4,3,2,1,0:T(2,128)(2,1)}, u32[]{:S(2)}) copy-start(bf16[8,128,2,2,128]{4,3,2,1,0:T(2,128)(2,1)} %reshape.96) | copy-start | bytes 3145732
  108.9 2.8 %copy-start.5 = (pred[8,128,512]{1,2,0:T(8,128)(4,1)S(1)}, pred[8,128,512]{1,2,0:T(8,128)(4,1)}, u32[]{:S(2)}) copy-start(pred[8,128,512]{1,2,0:T(8,128)(4,1)} %compare_and_fusion) | copy-start | bytes 1572868
  111.7 5.8 %copy-start.3 = (bf16[8,384,2,128]{1,3,2,0:T(8,128)(2,1)S(1)}, bf16[8,384,2,128]{1,3,2,0:T(8,128)(2,1)}, u32[]{:S(2)}) copy-start(bf16[8,384,2,128]{1,3,2,0:T(8,128)(2,1)} %copy.12) | copy-start | bytes 4718596
  111.7 5.8 %copy-start.4 = (bf16[8,128,2,128]{1,3,2,0:T(8,128)(2,1)S(1)}, bf16[8,128,2,128]{1,3,2,0:T(8,128)(2,1)}, u32[]{:S(2)}) copy-start(bf16[8,128,2,128]{1,3,2,0:T(8,128)(2,1)} %copy.11) | copy-start | bytes 1572868
Sparse Core Ops, SparseCore 0:
  127.0 48.4 reduce-scatter.1
where the time goes:
time: 186 us; the launch traced here: 182 us
  waiting for transfers between devices  61.1 us (33%)
  local copies, waits for them, and re-layouts  36.5 us (20%)
  matrix products  25.9 us (14%)
  blocking collectives  20.1 us (11%)
  starting transfers between devices  16.9 us (9%)
  between operations  13.5 us (7%)
  other arithmetic  8.31 us (4%)
    reduce_scatter x1, waiting for transfers between devices, shards(): lax.psum_scatter(jnp.dot(mixed, out_weight, preferred_element_type=jnp.fl...  48.6 us
    all_gather x1, blocking collectives, shards(): all_lists = lax.all_gather(chosen, 'kv', axis=0, tiled=True)  20.1 us
    all_to_all x1, waiting for transfers between devices, shards(): lax.all_to_all(key_rows[wanted], 'kv', split_axis=0, concat_axis=0, tiled...  12.4 us
    concatenate x4, local copies, waits for them, and re-layouts, shards(): jnp.concatenate([value_vectors.reshape(query_blocks, QUERY_BLOCK_SPAN, kv...  12.4 us
    concatenate x4, local copies, waits for them, and re-layouts, shards(): jnp.concatenate([key_vectors.reshape(query_blocks, QUERY_BLOCK_SPAN, kv_w...  10.3 us
    all_to_all x1, starting transfers between devices, shards(): lax.all_to_all(key_rows[wanted], 'kv', split_axis=0, concat_axis=0, tiled...  9.96 us
    all_to_all x1, starting transfers between devices, shards(): lax.all_to_all(value_rows[wanted], 'kv', split_axis=0, concat_axis=0, til...  6.97 us
    dot_general x1, matrix products, shards(): jnp.dot(tokens, query_weight, preferred_element_type=jnp.float32)  6.16 us
  transfers between devices with their start and end apart: 3, of which 2 were waited for; matrix products, arithmetic and copies ran while one was open for 19% of the time, Pallas kernels for 0%

commit v1 on v0

v1 whole, which is shorter than its diff:
```python
import functools

import jax
import jax.numpy as jnp
from jax import lax
from jax.experimental import pallas as pl
from jax.experimental.pallas import tpu as pltpu
from jax.sharding import PartitionSpec as P

HEAD = 128
QB = 128
KB = 32
PIECES = 4
ROWS = 256
BF = jnp.bfloat16
F32 = jnp.float32
MESH = pl.DeviceIdType.MESH


def block_pairs(blocks):
    half = blocks // 2
    firsts = list(range(0, half, 2)) + list(range(1, half, 2))
    return [(i, i + half) for i in firsts]


def kernel(
    nkv, ntp, nfar,
    tok_hbm, wq_hbm, wk_hbm, wv_hbm, wo_hbm, list_v, list_s,
    out_ref,
    tok, wq, wk, wv, wo, q, kv, att, attr, kall, tmine, trecv, tsm, stage, *rest,
):
    chunks = block_pairs(att.shape[0])
    nch = len(chunks)
    recv = rest[:nch]
    (loc_sem, tok_sem, ts_sem, tr_sem, tl_sem, zs_sem, zr_sem,
     as_sem, ar_sem, cs_sem, cr_sem, ys_sem, yr_sem, rs_sem, rr_sem) = rest[nch:]
    me = lax.axis_index("kv")
    tp = lax.axis_index("tp")
    blocks = att.shape[0]
    bpm = attr.shape[1]
    kvw = wk.shape[1]
    kv_heads = kvw // HEAD
    qw = wq.shape[1]
    group = qw // kvw
    bpg = kv.shape[0]
    steps = tok.shape[0] // ROWS
    per_step = ROWS // KB
    kd = wo.shape[1]
    ny = ntp // 2
    mate = tp + 1 - 2 * lax.rem(tp, 2)

    load_wk = pltpu.make_async_copy(wk_hbm, wk, loc_sem.at[0])
    load_wv = pltpu.make_async_copy(wv_hbm, wv, loc_sem.at[1])
    load_wq = pltpu.make_async_copy(wq_hbm, wq, loc_sem.at[2])
    load_wo = pltpu.make_async_copy(wo_hbm, wo.at[tp], loc_sem.at[3])

    def load_tok(s):
        rows = pl.ds(s * ROWS, ROWS)
        return pltpu.make_async_copy(tok_hbm.at[rows, :], tok.at[rows, :], tok_sem.at[s])

    load_wk.start()
    load_tok(0).start()
    load_wv.start()
    for s in range(1, steps):
        load_tok(s).start()

    barrier = pltpu.get_barrier_semaphore()

    def greet(i, c):
        other = lax.rem(me + i, nkv)
        pl.semaphore_signal(barrier, inc=1, device_id={"kv": other, "tp": tp}, device_id_type=MESH)
        return c

    lax.fori_loop(1, nkv, greet, 0)
    for i in range(1, ntp):
        pl.semaphore_signal(
            barrier, inc=1, device_id={"kv": me, "tp": lax.rem(tp + i, ntp)}, device_id_type=MESH
        )

    named = list_v[...]
    lane = lax.broadcasted_iota(jnp.int32, tmine.shape, 1)
    table = jnp.zeros(tmine.shape, jnp.int32)
    for p in range(nkv):
        local = named - p * bpg
        mine = (local >= 0) & (local < bpg)
        column = jnp.sum(jnp.where(mine, local, 0), axis=1, keepdims=True)
        table = jnp.where(lane == p, column, table)
    tmine[...] = table
    load_wq.start()
    load_wo.start()
    pl.semaphore_wait(barrier, nkv + ntp - 2)

    def table_copy(p):
        return pltpu.make_async_remote_copy(
            src_ref=tmine, dst_ref=trecv.at[me], send_sem=ts_sem.at[p], recv_sem=tr_sem.at[me],
            device_id={"kv": p, "tp": tp}, device_id_type=MESH,
        )

    def table_in(d):
        return pltpu.make_async_remote_copy(
            src_ref=tmine, dst_ref=trecv.at[d], send_sem=ts_sem.at[d], recv_sem=tr_sem.at[d],
            device_id={"kv": d, "tp": tp}, device_id_type=MESH,
        )

    def table_local(d):
        return pltpu.make_async_copy(trecv.at[d], tsm.at[d], tl_sem.at[d])

    def each(lower, upper, action):
        def body(i, c):
            action(i)
            return c

        lax.fori_loop(lower, upper, body, 0)

    each(0, me, lambda p: table_copy(p).start())

    piece = kd // PIECES
    mate_copy = pltpu.make_async_remote_copy(
        src_ref=wo_hbm, dst_ref=wo.at[tp], send_sem=cs_sem, recv_sem=cr_sem,
        device_id={"kv": me, "tp": mate}, device_id_type=MESH,
    )
    mate_in = pltpu.make_async_remote_copy(
        src_ref=wo_hbm, dst_ref=wo.at[mate], send_sem=cs_sem, recv_sem=cr_sem,
        device_id={"kv": me, "tp": mate}, device_id_type=MESH,
    )

    def far_copy(dy, i):
        rows = pl.ds(i * piece, piece)
        return pltpu.make_async_remote_copy(
            src_ref=wo_hbm.at[rows, :], dst_ref=wo.at[tp, rows, :],
            send_sem=ys_sem.at[dy, i], recv_sem=yr_sem.at[dy, i],
            device_id={"kv": me, "tp": lax.rem(tp + 2 * dy, ntp)}, device_id_type=MESH,
        )

    def relay(dy, i, owner):
        rows = pl.ds(i * piece, piece)
        return pltpu.make_async_remote_copy(
            src_ref=wo.at[owner, rows, :], dst_ref=wo.at[owner, rows, :],
            send_sem=rs_sem.at[dy, i], recv_sem=rr_sem.at[dy, i],
            device_id={"kv": me, "tp": mate}, device_id_type=MESH,
        )

    def sender_of(who, dy):
        return lax.rem(who - 2 * dy + ntp, ntp)

    def start_piece(i):
        for dy in range(1, ny):
            far_copy(dy, i).start()

    def relay_piece(i):
        for dy in range(1, ny):
            far_copy(dy, i).wait_recv()
            relay(dy, i, sender_of(tp, dy)).start()

    mate_copy.start()
    start_piece(0)
    start_piece(1)

    load_wk.wait()
    load_wv.wait()

    def project_kv(s):
        load_tok(s).wait()
        x = tok[pl.ds(s * ROWS, ROWS), :]
        k = jnp.dot(x, wk[...], preferred_element_type=F32).astype(BF)
        v = jnp.dot(x, wv[...], preferred_element_type=F32).astype(BF)
        where = pl.ds(s * per_step, per_step)
        kv[where, :, :kvw] = k.reshape(per_step, KB, kvw)
        kv[where, :, kvw:] = v.reshape(per_step, KB, kvw)

    each(0, steps, project_kv)

    def table_got(d):
        table_in(d).wait_recv()
        table_local(d).start()

    each(me + 1, nkv, table_got)
    each(me + 1, nkv, lambda d: table_local(d).wait())

    def send_copy(c, d):
        return pltpu.make_async_remote_copy(
            src_ref=stage.at[c, d], dst_ref=recv[c].at[me],
            send_sem=zs_sem.at[c, d], recv_sem=zr_sem.at[c, me],
            device_id={"kv": d, "tp": tp}, device_id_type=MESH,
        )

    def arrive(c, p):
        return pltpu.make_async_remote_copy(
            src_ref=stage.at[c, p], dst_ref=recv[c].at[p],
            send_sem=zs_sem.at[c, p], recv_sem=zr_sem.at[c, p],
            device_id={"kv": p, "tp": tp}, device_id_type=MESH,
        )

    later = nkv - 1 - me
    for c, pair in enumerate(chunks):

        def stage_one(i, c=c, pair=pair):
            d = nkv - 1 - i
            for slot, b in enumerate(pair):
                stage[c, d, slot] = kv[tsm[d, b, me]]

        each(0, later, stage_one)
        each(0, later, lambda i, c=c: send_copy(c, nkv - 1 - i).start())

    load_wq.wait()

    def project_q(s):
        rows = pl.ds(s * ROWS, ROWS)
        q[rows, :] = jnp.dot(tok[rows, :], wq[...], preferred_element_type=F32).astype(BF)

    each(0, steps, project_q)

    keys = kall.shape[1]
    used = QB + nfar * KB
    row = lax.broadcasted_iota(jnp.int32, (QB, keys), 0)
    col = lax.broadcasted_iota(jnp.int32, (QB, keys), 1)
    count = jnp.minimum(nfar, me)
    allowed = (col <= row) | ((col >= QB) & (col < QB + KB * count))
    allowed = jnp.concatenate([allowed.astype(jnp.int32)] * group, axis=0) > 0
    if keys > used:
        for slot in range(len(chunks[0])):
            kall[slot, used:, :] = jnp.zeros((keys - used, 2 * kvw), BF)
    scale = HEAD ** (-0.5)

    def attend(b, slot):
        parts = []
        for g in range(kv_heads):
            first = g * group
            qs = jnp.concatenate(
                [q[b * QB:(b + 1) * QB, (first + r) * HEAD:(first + r + 1) * HEAD] for r in range(group)],
                axis=0,
            )
            ks = kall[slot, :, g * HEAD:(g + 1) * HEAD]
            vs = kall[slot, :, kvw + g * HEAD:kvw + (g + 1) * HEAD]
            s = lax.dot_general(qs, ks, (((1,), (1,)), ((), ())), preferred_element_type=F32) * scale
            s = jnp.where(allowed, s, -jnp.inf)
            e = jnp.exp(s - jnp.max(s, axis=-1, keepdims=True))
            w = (e * (1.0 / jnp.sum(e, axis=-1, keepdims=True))).astype(BF)
            o = jnp.dot(w, vs, preferred_element_type=F32).astype(BF)
            for r in range(group):
                parts.append(o[r * QB:(r + 1) * QB, :])
        return jnp.concatenate(parts, axis=1)

    def att_copy(b):
        member, slot = b // bpm, b % bpm
        return pltpu.make_async_remote_copy(
            src_ref=att.at[b], dst_ref=attr.at[tp, slot],
            send_sem=as_sem.at[b], recv_sem=ar_sem.at[tp, slot],
            device_id={"kv": me, "tp": member}, device_id_type=MESH,
        )

    def att_in(t, slot):
        return pltpu.make_async_remote_copy(
            src_ref=att.at[slot], dst_ref=attr.at[t, slot],
            send_sem=as_sem.at[slot], recv_sem=ar_sem.at[t, slot],
            device_id={"kv": me, "tp": t}, device_id_type=MESH,
        )

    for c, pair in enumerate(chunks):
        each(0, me, lambda p, c=c: arrive(c, p).wait_recv())
        for slot, b in enumerate(pair):
            kall[slot, :QB, :] = kv[b * (QB // KB):(b + 1) * (QB // KB)].reshape(QB, 2 * kvw)
            for j in range(nfar):
                owner = jnp.where(j < count, list_s[b, j] // bpg, 0)
                block = recv[c][owner, slot]
                kall[slot, QB + j * KB:QB + (j + 1) * KB, :] = jnp.where(j < count, block, jnp.zeros_like(block))
        for slot, b in enumerate(pair):
            member = b // bpm
            result = attend(b, slot)
            att[b] = result

            @pl.when(tp == member)
            def _(result=result, b=b):
                attr[tp, b % bpm] = result

        for b in pair:
            @pl.when(tp != b // bpm)
            def _(b=b):
                att_copy(b).start()

        if c + 2 < PIECES:
            start_piece(c + 2)
        if c == 1:
            relay_piece(0)
            relay_piece(1)
        if c > 1:
            relay_piece(c)
    for i in range(nch, PIECES):
        relay_piece(i)

    load_wo.wait()
    mate_in.wait_recv()
    for i in range(PIECES):
        for dy in range(1, ny):
            relay(dy, i, sender_of(mate, dy)).wait_recv()
    for slot in range(bpm):
        for i in range(1, ntp):
            att_in(lax.rem(tp + i, ntp), slot).wait_recv()

    width = out_ref.shape[1]
    tile = min(512, width)

    def project_out(n):
        cols = pl.ds(pl.multiple_of(n * tile, tile), tile)
        total = jnp.zeros((bpm * QB, tile), F32)
        for t in range(ntp):
            a = attr[t].reshape(bpm * QB, kd)
            part = jnp.dot(a, wo[t, :, cols], preferred_element_type=F32)
            total = total + part.astype(BF).astype(F32)
        out_ref[:, cols] = total.astype(BF)

    each(0, width // tile, project_out)

    each(0, me, lambda p: table_copy(p).wait_send())
    for c in range(nch):
        each(me + 1, nkv, lambda d, c=c: send_copy(c, d).wait_send())
    mate_copy.wait_send()
    for i in range(PIECES):
        for dy in range(1, ny):
            far_copy(dy, i).wait_send()
            relay(dy, i, sender_of(tp, dy)).wait_send()
    for b in range(blocks):
        @pl.when(tp != b // bpm)
        def _(b=b):
            att_copy(b).wait_send()


def shards(nkv, ntp, tokens, wq, wk, wv, wo, chosen):
    rows, width = tokens.shape
    qw, kvw, kd = wq.shape[1], wk.shape[1], wo.shape[0]
    out_width = wo.shape[1]
    blocks = rows // QB
    nfar = min(chosen.shape[1], nkv - 1)
    bpm = rows // ntp // QB
    keys = -(-(QB + nfar * KB) // 128) * 128
    nch = blocks // 2
    dma = pltpu.SemaphoreType.DMA
    any_spec = pl.BlockSpec(memory_space=pl.ANY)
    return pl.pallas_call(
        functools.partial(kernel, nkv, ntp, nfar),
        out_shape=jax.ShapeDtypeStruct((rows // ntp, out_width), BF),
        in_specs=[any_spec] * 5
        + [pl.BlockSpec(memory_space=pltpu.VMEM), pl.BlockSpec(memory_space=pltpu.SMEM)],
        out_specs=pl.BlockSpec(memory_space=pltpu.VMEM),
        scratch_shapes=[
            pltpu.VMEM((rows, width), BF),
            pltpu.VMEM((width, qw), BF),
            pltpu.VMEM((width, kvw), BF),
            pltpu.VMEM((width, kvw), BF),
            pltpu.VMEM((ntp, kd, out_width), BF),
            pltpu.VMEM((rows, qw), BF),
            pltpu.VMEM((rows // KB, KB, 2 * kvw), BF),
            pltpu.VMEM((blocks, QB, qw), BF),
            pltpu.VMEM((ntp, bpm, QB, qw), BF),
            pltpu.VMEM((2, keys, 2 * kvw), BF),
            pltpu.VMEM((blocks, 128), jnp.int32),
            pltpu.VMEM((nkv, blocks, 128), jnp.int32),
            pltpu.SMEM((nkv, blocks, 128), jnp.int32),
            pltpu.VMEM((nch, nkv, 2, KB, 2 * kvw), BF),
        ]
        + [pltpu.VMEM((nkv, 2, KB, 2 * kvw), BF)] * nch
        + [
            dma((4,)), dma((rows // ROWS,)), dma((nkv,)), dma((nkv,)), dma((nkv,)),
            dma((nch, nkv)), dma((nch, nkv)), dma((blocks,)), dma((ntp, bpm)),
            dma, dma,
            dma((ntp // 2, PIECES)), dma((ntp // 2, PIECES)),
            dma((ntp // 2, PIECES)), dma((ntp // 2, PIECES)),
        ],
        compiler_params=pltpu.CompilerParams(
            collective_id=1, has_side_effects=True, vmem_limit_bytes=58 << 20
        ),
    )(tokens, wq, wk, wv, wo, chosen, chosen)


def solution(mesh):
    return jax.shard_map(
        functools.partial(shards, mesh.shape["kv"], mesh.shape["tp"]),
        mesh=mesh,
        in_specs=(
            P("kv", None),
            P(None, "tp"),
            P(None, "tp"),
            P(None, "tp"),
            P("tp", None),
            P("kv", None),
        ),
        out_specs=P(("kv", "tp"), None),
        check_vma=False,
    )
```

time: 186 us -> 73.4 us (0.39); the launches traced: 182 us -> 72.2 us
  Pallas kernels: 0 us -> 69.8 us
  waiting for transfers between devices: 61.1 us -> 0 us
  local copies, waits for them, and re-layouts: 36.5 us -> 2.3 us
  matrix products: 25.9 us -> 0 us
  blocking collectives: 20.1 us -> 0 us
  starting transfers between devices: 16.9 us -> 0 us
  between operations: 13.5 us -> 0.01 us
  other arithmetic: 8.31 us -> 0 us
    pallas_call x0 -> x1, Pallas kernels: none -> 69.8 us  [shards(): pl.pallas_call(functools.partial(kernel, nkv, ntp, nfar), out_shape=jax.S...]
    reduce_scatter x1 -> x0, waiting for transfers between devices: 48.6 us -> none  [shards(): lax.psum_scatter(jnp.dot(mixed, out_weight, preferred_element_type=jnp.fl...]
    dot_general x6 -> x0, matrix products: 25.9 us -> none  [the longest x1 6.16 us: shards(): jnp.dot(tokens, query_weight, preferred_element_type=jnp.float32)]
    concatenate x10 -> x0, local copies, waits for them, and re-layouts: 22.8 us -> none  [the longest x4 12.4 us: shards(): jnp.concatenate([value_vectors.reshape(query_blocks, QUERY_BLOCK_SPAN, kv...]
    all_gather x1 -> x0, blocking collectives: 20.1 us -> none  [shards(): all_lists = lax.all_gather(chosen, 'kv', axis=0, tiled=True)]
    all_to_all x2 -> x0, starting transfers between devices: 16.9 us -> none  [the longest x1 9.96 us: shards(): lax.all_to_all(key_rows[wanted], 'kv', split_axis=0, concat_axis=0, tiled...]
    all_to_all x2 -> x0, waiting for transfers between devices: 12.4 us -> none  [the longest x1 12.4 us: shards(): lax.all_to_all(key_rows[wanted], 'kv', split_axis=0, concat_axis=0, tiled...]
    gather x4 -> x0, local copies, waits for them, and re-layouts: 10.2 us -> none  [the longest x1 3.64 us: shards(): far_values = received[1][owners, block_slot]]
  transfers between devices with their start and end apart: 3 -> 0, of which waited for: 2 -> 0; matrix products, arithmetic and copies ran while one was open for 19% -> 0% of each run, Pallas kernels for 0% -> 0%
where the time goes in v1:
time: 73.4 us; the launch traced here: 72.2 us
  Pallas kernels  69.8 us (95%)
  local copies, waits for them, and re-layouts  2.3 us (3%)
    pallas_call x1, Pallas kernels, shards(): pl.pallas_call(functools.partial(kernel, nkv, ntp, nfar), out_shape=jax.S...  69.8 us
    unnamed x1, local copies, waits for them, and re-layouts  2.3 us

profile of v1, /device:TPU:21, one launch (start us, length us, event | category | flops | bytes accessed | tf_op | source)
XLA Modules:
  0.0 72.2 jit_solution(10772151940868570074)
XLA Ops:
  0.0 69.8 %shard_map.64 = bf16[256,2048]{1,0:T(8,128)(2,1)} custom-call(bf16[1024,2048]{1,0:T(8,128)(2,1)} %tok_hbm.1, bf16[2048,512]{1,0:T(8,128)(2,1)} %wq_hbm.1, bf16[2048,256]{1,0:T(8,128)(2,1)} %wk_hbm.1, bf16[2048,256]{1,0:T(8,128)(2,1)} %wv_hbm.1, bf16[512,2048]{1,0:T(8,128)(2,1)} %wo_hbm.1, s32[8,12]{1,0:T(8,128)} %list_s.1, s32[8,12]{1,0:T(8,128)} %list_s.1), custom_call_target="tpu_custom_call" | custom-call | tf_op jit(solution)/shard_map/pallas_call | solution.py:339
  69.8 2.3 %copy.8 = bf16[256,2048]{1,0:T(8,128)(2,1)} copy(bf16[256,2048]{1,0:T(8,128)(2,1)} %shard_map.64) | data formatting | bytes 2097152

commit v2 on v1

--- a/solution.py
+++ b/solution.py
@@ -14,26 +14,28 @@
 ROWS = 256
 BF = jnp.bfloat16
 F32 = jnp.float32
+LOG2E = 1.4426950408889634
 MESH = pl.DeviceIdType.MESH
 
 
 def block_pairs(blocks):
     half = blocks // 2
     firsts = list(range(0, half, 2)) + list(range(1, half, 2))
-    return [(i, i + half) for i in firsts]
+    pairs = [(i, i + half) for i in firsts]
+    return pairs[:-1] + [(b,) for b in pairs[-1]]
 
 
 def kernel(
     nkv, ntp, nfar,
     tok_hbm, wq_hbm, wk_hbm, wv_hbm, wo_hbm, list_v, list_s,
     out_ref,
-    tok, wq, wk, wv, wo, q, kv, att, attr, kall, tmine, trecv, tsm, stage, *rest,
+    tok, wq, wk, wv, wo, q, kv, att, attr, kall, tmine, trecv, tsm, bias, stage, *rest,
 ):
     chunks = block_pairs(att.shape[0])
     nch = len(chunks)
     recv = rest[:nch]
     (loc_sem, tok_sem, ts_sem, tr_sem, tl_sem, zs_sem, zr_sem,
-     as_sem, ar_sem, cs_sem, cr_sem, ys_sem, yr_sem, rs_sem, rr_sem) = rest[nch:]
+     as_sem, ar_sem, cs_sem, cr_sem, ys_sem, yr_sem, rs_sem, rr_sem, xs_sem, xr_sem) = rest[nch:]
     me = lax.axis_index("kv")
     tp = lax.axis_index("tp")
     blocks = att.shape[0]
@@ -86,8 +88,6 @@
         column = jnp.sum(jnp.where(mine, local, 0), axis=1, keepdims=True)
         table = jnp.where(lane == p, column, table)
     tmine[...] = table
-    load_wq.start()
-    load_wo.start()
     pl.semaphore_wait(barrier, nkv + ntp - 2)
 
     def table_copy(p):
@@ -124,16 +124,34 @@
         device_id={"kv": me, "tp": mate}, device_id_type=MESH,
     )
 
+    parity = lax.rem(me, 2)
+    across = me + 1 - 2 * parity
+
+    def piece_rows(i):
+        if i == 2:
+            i = 2 + parity
+        elif i == 3:
+            i = 3 - parity
+        return pl.ds(pl.multiple_of(i * piece, piece), piece)
+
     def far_copy(dy, i):
-        rows = pl.ds(i * piece, piece)
+        rows = piece_rows(i)
         return pltpu.make_async_remote_copy(
             src_ref=wo_hbm.at[rows, :], dst_ref=wo.at[tp, rows, :],
             send_sem=ys_sem.at[dy, i], recv_sem=yr_sem.at[dy, i],
             device_id={"kv": me, "tp": lax.rem(tp + 2 * dy, ntp)}, device_id_type=MESH,
         )
 
+    def across_copy(dy, i):
+        owner, rows = sender_of(tp, dy), piece_rows(i)
+        return pltpu.make_async_remote_copy(
+            src_ref=wo.at[owner, rows, :], dst_ref=wo.at[owner, rows, :],
+            send_sem=xs_sem.at[dy], recv_sem=xr_sem.at[dy],
+            device_id={"kv": across, "tp": tp}, device_id_type=MESH,
+        )
+
     def relay(dy, i, owner):
-        rows = pl.ds(i * piece, piece)
+        rows = piece_rows(i)
         return pltpu.make_async_remote_copy(
             src_ref=wo.at[owner, rows, :], dst_ref=wo.at[owner, rows, :],
             send_sem=rs_sem.at[dy, i], recv_sem=rr_sem.at[dy, i],
@@ -149,12 +167,16 @@
 
     def relay_piece(i):
         for dy in range(1, ny):
-            far_copy(dy, i).wait_recv()
+            if i == 3:
+                across_copy(dy, 3).wait_recv()
+            else:
+                far_copy(dy, i).wait_recv()
+            if i == 2:
+                across_copy(dy, 2).start()
             relay(dy, i, sender_of(tp, dy)).start()
 
-    mate_copy.start()
-    start_piece(0)
-    start_piece(1)
+    for i in (2, 0, 1):
+        start_piece(i)
 
     load_wk.wait()
     load_wv.wait()
@@ -179,18 +201,19 @@
 
     def send_copy(c, d):
         return pltpu.make_async_remote_copy(
-            src_ref=stage.at[c, d], dst_ref=recv[c].at[me],
+            src_ref=stage.at[c, d, pl.ds(0, len(chunks[c]))], dst_ref=recv[c].at[me],
             send_sem=zs_sem.at[c, d], recv_sem=zr_sem.at[c, me],
             device_id={"kv": d, "tp": tp}, device_id_type=MESH,
         )
 
     def arrive(c, p):
         return pltpu.make_async_remote_copy(
-            src_ref=stage.at[c, p], dst_ref=recv[c].at[p],
+            src_ref=stage.at[c, p, pl.ds(0, len(chunks[c]))], dst_ref=recv[c].at[p],
             send_sem=zs_sem.at[c, p], recv_sem=zr_sem.at[c, p],
             device_id={"kv": p, "tp": tp}, device_id_type=MESH,
         )
 
+    load_wq.start()
     later = nkv - 1 - me
     for c, pair in enumerate(chunks):
 
@@ -202,6 +225,8 @@
         each(0, later, stage_one)
         each(0, later, lambda i, c=c: send_copy(c, nkv - 1 - i).start())
 
+    load_wo.start()
+    mate_copy.start()
     load_wq.wait()
 
     def project_q(s):
@@ -216,11 +241,13 @@
     col = lax.broadcasted_iota(jnp.int32, (QB, keys), 1)
     count = jnp.minimum(nfar, me)
     allowed = (col <= row) | ((col >= QB) & (col < QB + KB * count))
-    allowed = jnp.concatenate([allowed.astype(jnp.int32)] * group, axis=0) > 0
+    allowed = jnp.where(allowed, 0.0, -jnp.inf)
+    for r in range(group):
+        bias[r * QB:(r + 1) * QB, :] = allowed
     if keys > used:
         for slot in range(len(chunks[0])):
             kall[slot, used:, :] = jnp.zeros((keys - used, 2 * kvw), BF)
-    scale = HEAD ** (-0.5)
+    scale = HEAD ** (-0.5) * LOG2E
 
     def attend(b, slot):
         parts = []
@@ -233,8 +260,8 @@
             ks = kall[slot, :, g * HEAD:(g + 1) * HEAD]
             vs = kall[slot, :, kvw + g * HEAD:kvw + (g + 1) * HEAD]
             s = lax.dot_general(qs, ks, (((1,), (1,)), ((), ())), preferred_element_type=F32) * scale
-            s = jnp.where(allowed, s, -jnp.inf)
-            e = jnp.exp(s - jnp.max(s, axis=-1, keepdims=True))
+            s = s + bias[...]
+            e = jnp.exp2(s - jnp.max(s, axis=-1, keepdims=True))
             w = (e * (1.0 / jnp.sum(e, axis=-1, keepdims=True))).astype(BF)
             o = jnp.dot(w, vs, preferred_element_type=F32).astype(BF)
             for r in range(group):
@@ -255,6 +282,33 @@
             send_sem=as_sem.at[slot], recv_sem=ar_sem.at[t, slot],
             device_id={"kv": me, "tp": t}, device_id_type=MESH,
         )
+
+    def weights_here():
+        load_wo.wait()
+        mate_in.wait_recv()
+        for i in range(PIECES):
+            for dy in range(1, ny):
+                relay(dy, i, sender_of(mate, dy)).wait_recv()
+
+    width = out_ref.shape[1]
+    tile = min(512, width)
+
+    def early(slot):
+        return max(c for c, pair in enumerate(chunks) for b in pair if b % bpm == slot) <= nch - 3
+
+    def finish(slot):
+        for i in range(1, ntp):
+            att_in(lax.rem(tp + i, ntp), slot).wait_recv()
+
+        def project_out(n):
+            cols = pl.ds(pl.multiple_of(n * tile, tile), tile)
+            total = jnp.zeros((QB, tile), F32)
+            for t in range(ntp):
+                part = jnp.dot(attr[t, slot], wo[t, :, cols], preferred_element_type=F32)
+                total = total + part.astype(BF).astype(F32)
+            out_ref[slot * QB:(slot + 1) * QB, cols] = total.astype(BF)
+
+        each(0, width // tile, project_out)
 
     for c, pair in enumerate(chunks):
         each(0, me, lambda p, c=c: arrive(c, p).wait_recv())
@@ -278,38 +332,22 @@
             def _(b=b):
                 att_copy(b).start()
 
-        if c + 2 < PIECES:
-            start_piece(c + 2)
+        if c == 0:
+            relay_piece(2)
         if c == 1:
             relay_piece(0)
+        if c == nch - 3:
             relay_piece(1)
-        if c > 1:
-            relay_piece(c)
-    for i in range(nch, PIECES):
-        relay_piece(i)
-
-    load_wo.wait()
-    mate_in.wait_recv()
-    for i in range(PIECES):
-        for dy in range(1, ny):
-            relay(dy, i, sender_of(mate, dy)).wait_recv()
+            relay_piece(3)
+        if c == nch - 2:
+            weights_here()
+            for slot in range(bpm):
+                if early(slot):
+                    finish(slot)
+
     for slot in range(bpm):
-        for i in range(1, ntp):
-            att_in(lax.rem(tp + i, ntp), slot).wait_recv()
-
-    width = out_ref.shape[1]
-    tile = min(512, width)
-
-    def project_out(n):
-        cols = pl.ds(pl.multiple_of(n * tile, tile), tile)
-        total = jnp.zeros((bpm * QB, tile), F32)
-        for t in range(ntp):
-            a = attr[t].reshape(bpm * QB, kd)
-            part = jnp.dot(a, wo[t, :, cols], preferred_element_type=F32)
-            total = total + part.astype(BF).astype(F32)
-        out_ref[:, cols] = total.astype(BF)
-
-    each(0, width // tile, project_out)
+        if not early(slot):
+            finish(slot)
 
     each(0, me, lambda p: table_copy(p).wait_send())
     for c in range(nch):
@@ -317,7 +355,10 @@
     mate_copy.wait_send()
     for i in range(PIECES):
         for dy in range(1, ny):
-            far_copy(dy, i).wait_send()
+            if i < 3:
+                far_copy(dy, i).wait_send()
+            if i == 2:
+                across_copy(dy, 2).wait_send()
             relay(dy, i, sender_of(tp, dy)).wait_send()
     for b in range(blocks):
         @pl.when(tp != b // bpm)
@@ -333,9 +374,11 @@
     nfar = min(chosen.shape[1], nkv - 1)
     bpm = rows // ntp // QB
     keys = -(-(QB + nfar * KB) // 128) * 128
-    nch = blocks // 2
+    chunks = block_pairs(blocks)
+    nch = len(chunks)
+    group = qw // kvw
     dma = pltpu.SemaphoreType.DMA
-    any_spec = pl.BlockSpec(memory_space=pl.ANY)
+    any_spec = pl.BlockSpec(memory_space=pltpu.HBM)
     return pl.pallas_call(
         functools.partial(kernel, nkv, ntp, nfar),
         out_shape=jax.ShapeDtypeStruct((rows // ntp, out_width), BF),
@@ -356,18 +399,20 @@
             pltpu.VMEM((blocks, 128), jnp.int32),
             pltpu.VMEM((nkv, blocks, 128), jnp.int32),
             pltpu.SMEM((nkv, blocks, 128), jnp.int32),
+            pltpu.VMEM((group * QB, keys), F32),
             pltpu.VMEM((nch, nkv, 2, KB, 2 * kvw), BF),
         ]
-        + [pltpu.VMEM((nkv, 2, KB, 2 * kvw), BF)] * nch
+        + [pltpu.VMEM((nkv, len(pair), KB, 2 * kvw), BF) for pair in chunks]
         + [
             dma((4,)), dma((rows // ROWS,)), dma((nkv,)), dma((nkv,)), dma((nkv,)),
             dma((nch, nkv)), dma((nch, nkv)), dma((blocks,)), dma((ntp, bpm)),
             dma, dma,
             dma((ntp // 2, PIECES)), dma((ntp // 2, PIECES)),
             dma((ntp // 2, PIECES)), dma((ntp // 2, PIECES)),
+            dma((ntp // 2,)), dma((ntp // 2,)),
         ],
         compiler_params=pltpu.CompilerParams(
-            collective_id=1, has_side_effects=True, vmem_limit_bytes=58 << 20
+            collective_id=1, has_side_effects=True, vmem_limit_bytes=52 << 20
         ),
     )(tokens, wq, wk, wv, wo, chosen, chosen)
 

time: 73.4 us -> 66.1 us (0.901); the launches traced: 72.2 us -> 65.9 us
  Pallas kernels: 69.8 us -> 64.3 us
    pallas_call x1, Pallas kernels: 69.8 us -> 64.3 us  [shards(): pl.pallas_call(functools.partial(kernel, nkv, ntp, nfar), out_shape=jax.S...]
    unnamed x1 -> x3, local copies, waits for them, and re-layouts: 2.3 us -> 1.66 us
where the time goes in v2:
time: 66.1 us; the launch traced here: 65.9 us
  Pallas kernels  64.3 us (97%)
  local copies, waits for them, and re-layouts  1.66 us (3%)
    pallas_call x1, Pallas kernels, shards(): pl.pallas_call(functools.partial(kernel, nkv, ntp, nfar), out_shape=jax.S...  64.3 us
    unnamed x3, local copies, waits for them, and re-layouts  1.66 us

profile of v2, /device:TPU:21, one launch (start us, length us, event | category | flops | bytes accessed | tf_op | source)
XLA Modules:
  0.0 65.9 jit_solution(14557792961014605985)
XLA Ops:
  0.0 0.0 copy-start
  0.0 0.7 %copy-done = s32[8,12]{1,0:T(8,128)S(1)} copy-done((s32[8,12]{1,0:T(8,128)S(1)}, s32[8,12]{1,0:T(8,128)}, u32[]{:S(2)}) %copy-start) | copy-done | bytes 408
  0.7 64.3 %shard_map.64 = bf16[256,2048]{1,0:T(8,128)(2,1)S(1)} custom-call(bf16[1024,2048]{1,0:T(8,128)(2,1)} %tok_hbm.1, bf16[2048,512]{1,0:T(8,128)(2,1)} %wq_hbm.1, bf16[2048,256]{1,0:T(8,128)(2,1)} %wk_hbm.1, bf16[2048,256]{1,0:T(8,128)(2,1)} %wv_hbm.1, bf16[512,2048]{1,0:T(8,128)(2,1)} %wo_hbm.1, s32[8,12]{1,0:T(8,128)S(1)} %copy-done, s32[8,12]{1,0:T(8,128)S(1)} %copy-done), custom_call_target="tpu_custom_call" | custom-call | tf_op jit(solution)/shard_map/pallas_call | solution.py:382
  65.0 1.0 %copy.8 = bf16[256,2048]{1,0:T(8,128)(2,1)} copy(bf16[256,2048]{1,0:T(8,128)(2,1)S(1)} %shard_map.64) | data formatting | bytes 2097152
Async XLA Ops:
  0.0 0.7 %copy-start = (s32[8,12]{1,0:T(8,128)S(1)}, s32[8,12]{1,0:T(8,128)}, u32[]{:S(2)}) copy-start(s32[8,12]{1,0:T(8,128)} %list_s.1) | copy-start | bytes 1156
